TPU v7x, 32 devices: a whole 2x2x4 slice. The times are simulated.
32 devices in a mesh: grp: 2 (over y), fs: 4 (over z), tp: 4 (over x, core).
Axes of the slice: x: 2, y: 2, z: 4, core: 2. Of those that a mesh axis runs over, the one named last changes fastest.
Arguments:
- tokens: bfloat16 [2048, 2048], P(('grp', 'fs')), parts along dimension 0, may hold values from -6 to 6
- norm_gain: float32 [2048], P('fs'), may hold values from 0.1 to 1.9
- gate_master: float32 [4, 2048, 1024], P(None, 'fs', 'tp'), may hold values from -0.125 to 0.125
- up_master: float32 [4, 2048, 1024], P(None, 'fs', 'tp'), may hold values from -0.125 to 0.125
- chosen: int32 [2048, 2], P(('grp', 'fs')), parts along dimension 0, may hold values from 0 to 3, all different within a row; in each aligned block of 256 rows (0 to 255, 256 to 511, ...) at most 256 rows name the same one
- affinity: float32 [2048, 2], P(('grp', 'fs')), parts along dimension 0, may hold values from 0.05 to 1
Outputs:
- gate_served: bfloat16 [8, 2048, 1024], P(('grp', 'fs'), None, 'tp'), parts along dimension 0
- up_served: bfloat16 [8, 2048, 1024], P(('grp', 'fs'), None, 'tp'), parts along dimension 0
- hidden: bfloat16 [2048, 2, 1024], P(('grp', 'fs'), None, 'tp'), parts along dimension 0
There are 2 independent parts, one for each index of `grp`. A program takes and returns all parts, laid end to end along the dimension named above; an argument that names none is the same for every part. Nothing has to cross between parts.
Inputs may be any that keep to these rules, and one draw needn't show every extreme that they name: Among the rows of one index of fs (256 tokens, all their choices) no expert is chosen more than 256 times, a bound that some block reaches; the choices of one token differ.
All inputs are finite; a program needn't handle non-finite values.
Results may differ from a plain program's by a relative error of at most 0.023.
Values may be sent and summed in bfloat16 or wider, within the bound.
A program may use at most 64 MiB of HBM per device.

v0:
```python
import jax
import jax.numpy as jnp
from jax import lax
from jax.sharding import PartitionSpec as P


def on_device(tokens, norm_gain, gate_master, up_master, chosen, affinity):
    folded_gate = (gate_master * norm_gain[None, :, None]).astype(jnp.bfloat16)
    folded_up = (up_master * norm_gain[None, :, None]).astype(jnp.bfloat16)
    new_gate, new_up = (
        lax.all_to_all(folded_gate, "fs", split_axis=0, concat_axis=1, tiled=True),
        lax.all_to_all(folded_up, "fs", split_axis=0, concat_axis=1, tiled=True),
    )
    experts_all = gate_master.shape[0]
    tok_rows, width = tokens.shape
    top = chosen.shape[1]
    capacity = tok_rows * top * 2 // experts_all
    local = new_gate.shape[0]
    xfloat = tokens.astype(jnp.float32)
    scale = lax.rsqrt(jnp.mean(xfloat * xfloat, axis=-1) + 1e-06)
    share = affinity / jnp.sum(affinity, axis=-1, keepdims=True)
    flat_e = chosen.reshape(-1)
    onehot = (flat_e[:, None] == jnp.arange(experts_all, dtype=jnp.int32)[None, :]).astype(
        jnp.int32
    )
    slot = jnp.sum((jnp.cumsum(onehot, axis=0) - onehot) * onehot, axis=1)
    target = flat_e * capacity + slot
    owner = jnp.repeat(jnp.arange(tok_rows, dtype=jnp.int32), top)
    total = experts_all * capacity
    scale_buf = (
        jnp.zeros((total,), jnp.float32).at[target].set(scale[owner]).reshape(experts_all, capacity)
    )
    share_buf = (
        jnp.zeros((total,), jnp.float32)
        .at[target]
        .set(share.reshape(-1))
        .reshape(experts_all, capacity)
    )
    narrow = width // lax.axis_size("tp")
    own_cols = lax.dynamic_slice_in_dim(tokens, lax.axis_index("tp") * narrow, narrow, 1)
    row_buf = jnp.zeros((total, narrow), jnp.bfloat16).at[target].set(own_cols[owner])
    row_buf = row_buf.reshape(experts_all, capacity, narrow)
    got_rows, got_scale, got_share = (
        lax.all_to_all(row_buf, "fs", split_axis=0, concat_axis=0, tiled=True),
        lax.all_to_all(
            scale_buf.astype(jnp.bfloat16), "fs", split_axis=0, concat_axis=0, tiled=True
        ).astype(scale_buf.dtype),
        lax.all_to_all(
            share_buf.astype(jnp.bfloat16), "fs", split_axis=0, concat_axis=0, tiled=True
        ).astype(share_buf.dtype),
    )
    sources = got_rows.shape[0] // local
    got_rows = got_rows.reshape(sources, local, capacity, narrow)
    piece = lax.all_gather(got_rows, "tp", axis=3, tiled=True)
    more_gate = jnp.einsum("secd,edf->secf", piece, new_gate, preferred_element_type=jnp.float32)
    more_up = jnp.einsum("secd,edf->secf", piece, new_up, preferred_element_type=jnp.float32)
    gate = more_gate
    up = more_up
    factor = got_scale.reshape(sources, local, capacity)[..., None]
    weight = got_share.reshape(sources, local, capacity)[..., None]
    gate = gate * factor
    up = up * factor
    hidden_rows = (weight * jax.nn.silu(gate) * up).astype(jnp.bfloat16)
    hidden_rows = hidden_rows.reshape(sources * local, capacity, hidden_rows.shape[3])
    back = lax.all_to_all(hidden_rows, "fs", split_axis=0, concat_axis=0, tiled=True)
    picked = back.reshape(total, back.shape[2])[target].reshape(tok_rows, top, back.shape[2])
    return (new_gate, new_up, picked)


def solution(mesh):
    return jax.shard_map(
        on_device,
        mesh=mesh,
        in_specs=(
            P(("grp", "fs"), None),
            P("fs"),
            P(None, "fs", "tp"),
            P(None, "fs", "tp"),
            P(("grp", "fs"), None),
            P(("grp", "fs"), None),
        ),
        out_specs=(
            P(("grp", "fs"), None, "tp"),
            P(("grp", "fs"), None, "tp"),
            P(("grp", "fs"), None, "tp"),
        ),
        check_vma=False,
    )
```

profile of v0, /device:TPU:0, one launch (start us, length us, event | category | flops | bytes accessed | tf_op | source)
XLA Modules:
  0.0 163.8 jit_solution(18356809726918053598)
XLA Ops:
  7.2 0.0 all-gather.3.cloned.1.call-start
  7.2 0.7 broadcast_multiply_fusion
  7.9 0.8 copy.26
  8.7 0.1 eq.29
  8.9 0.1 eq.25
  9.0 0.1 copy.25
  9.1 0.1 mul.75
  9.3 1.2 reduce-window.6
  10.5 0.2 slice_reduce_fusion
  10.8 0.2 reduce-window.9
  10.9 0.1 add_bitcast_fusion
  11.0 0.1 reshape.174
  11.2 1.0 constant_dynamic-slice_fusion
  12.2 0.0 copy-start.1
  12.2 0.0 copy-start
  12.2 5.0 %scatter_custom_fusion.1 = bf16[1024,512]{1,0:T(8,128)(2,1)S(1)} fusion(s32[512]{0:T(512)S(1)} %bitcast.83, bf16[256,512]{1,0:T(8,128)(2,1)S(1)} %constant_dynamic-slice_fusion, s32[1024]{0:T(1024)S(1)} %pad_clamp_fusion.1, bf16[]{:T(256)} %constant.15.clone.1), kind=kCustom, calls=%fused_computation.18 | custom fusion | bytes 1048578 | tf_op jit(solution)/shard_map/scatter | solution.py:41
  17.3 32.0 %all_to_all.46 = bf16[4,256,512]{2,1,0:T(8,128)(2,1)} all-to-all(bf16[4,256,512]{2,1,0:T(8,128)(2,1)S(1)} %bitcast.82), channel_id=1, replica_groups=mesh['grp'=2,'fs'=4,'tp'=4] {'fs'}, dimensions={0} | all-to-all | bytes 2097152 | tf_op jit(solution)/shard_map/all_to_all | solution.py:44
  49.3 0.0 copy-start.2
  49.3 0.0 all-gather.3.cloned.1.call-update
  49.3 0.0 copy-done.1
  49.3 0.1 copy.28
  49.5 0.1 reshape.212
  49.6 2.4 %scatter_custom_fusion = f32[1024]{0:T(1024)S(1)} fusion(s32[512]{0:T(512)S(1)} %bitcast.84, f32[512]{0:T(512)S(1)} %reshape.212, f32[]{:T(128)} %constant.11.clone.1), kind=kCustom, calls=%fused_computation.38 | custom fusion | bytes 4100 | tf_op jit(solution)/shard_map/scatter | solution.py:36
  52.1 0.5 broadcast.103
  52.6 0.7 reduce.3
  53.3 0.6 reshape.249
  53.9 3.2 %all-to-all-start.2 = ((bf16[4,2,128]{2,1,0:T(2,128)(2,1)}), bf16[4,2,128]{2,1,0:T(2,128)(2,1)S(1)}, u32[]{:S(2)}, u32[]{:S(2)}) async-start(bf16[4,2,128]{2,1,0:T(2,128)(2,1)} %reshape.249), calls=%async_computation.2 | async-start | bytes 4096 | tf_op jit(solution)/shard_map/all_to_all | solution.py:48
  57.1 0.0 copy-done
  57.1 0.3 multiply_reduce_fusion
  57.4 3.5 %gather_fusion = f32[512]{0:T(512)S(1)} fusion(f32[256]{0:T(256)S(1)} %add_rsqrt_fusion, s32[1024]{0:T(1024)S(1)} %pad_clamp_fusion.1), kind=kCustom, calls=%fused_computation.1 | custom fusion | bytes 6144 | tf_op jit(solution)/shard_map/gather | solution.py:31
  61.0 2.4 %scatter_custom_fusion.2 = f32[1024]{0:T(1024)S(1)} fusion(s32[512]{0:T(512)S(1)} %bitcast.85, f32[512]{0:T(512)S(1)} %gather_fusion, f32[]{:T(128)} %constant.11.clone.1), kind=kCustom, calls=%fused_computation.36 | custom fusion | bytes 4100 | tf_op jit(solution)/shard_map/scatter | solution.py:31
  63.4 0.7 reduce.2
  64.1 0.6 reshape.247
  64.7 0.0 all-to-all-done.2
  64.7 5.0 %all-to-all-start.4 = ((bf16[4,2,128]{2,1,0:T(2,128)(2,1)}), bf16[4,2,128]{2,1,0:T(2,128)(2,1)S(1)}, u32[]{:S(2)}, u32[]{:S(2)}) async-start(bf16[4,2,128]{2,1,0:T(2,128)(2,1)} %reshape.247), calls=%async_computation.4 | async-start | bytes 4096 | tf_op jit(solution)/shard_map/all_to_all | solution.py:45
  69.7 0.0 copy-done.2
  69.7 3.5 %multiply_convert_fusion = (bf16[4,512,256]{2,1,0:T(8,128)(2,1)}, bf16[4,512,256]{2,1,0:T(8,128)(2,1)S(1)}) fusion(f32[4,512,256]{2,1,0:T(8,128)} %param.9, f32[512]{0:T(512)S(1)} %copy-done.2, f32[4,512,256]{2,1,0:T(8,128)} %param.8), kind=kLoop, calls=%fused_computation.7 | loop fusion | flops 2097152 | bytes 6293504 | tf_op jit(solution)/shard_map/convert_element_type | solution.py:9
  73.3 2.0 %all-to-all-done.4 = bf16[4,2,128]{2,1,0:T(2,128)(2,1)S(1)} async-done(((bf16[4,2,128]{2,1,0:T(2,128)(2,1)}), bf16[4,2,128]{2,1,0:T(2,128)(2,1)S(1)}, u32[]{:S(2)}, u32[]{:S(2)}) %all-to-all-start.4) | async-done | bytes 2080 | tf_op jit(solution)/shard_map/all_to_all | solution.py:45
  75.2 26.7 %all_to_all.47 = bf16[4,512,256]{2,1,0:T(8,128)(2,1)S(1)} all-to-all(bf16[4,512,256]{2,1,0:T(8,128)(2,1)S(1)} %get-tuple-element.4), channel_id=1, replica_groups=mesh['grp'=2,'fs'=4,'tp'=4] {'fs'}, dimensions={0} | all-to-all | bytes 2097152 | tf_op jit(solution)/shard_map/all_to_all | solution.py:11
  101.9 3.7 %all-to-all-start.1 = ((bf16[4,512,256]{2,1,0:T(8,128)(2,1)}), bf16[4,512,256]{2,1,0:T(8,128)(2,1)S(1)}, u32[]{:S(2)}, u32[]{:S(2)}) async-start(bf16[4,512,256]{2,1,0:T(8,128)(2,1)} %get-tuple-element.3), calls=%async_computation.1 | async-start | bytes 2097152 | tf_op jit(solution)/shard_map/all_to_all | solution.py:12
  105.7 0.0 all-gather.3.cloned.1.call-done
  105.7 3.5 %fusion.3 = f32[4,1,256,256]{2,3,0,1:T(8,128)S(1)} fusion(bf16[2048,256,1]{1,0,2:T(8,128)(2,1)S(1)} %bitcast.78, bf16[4,256,2048]{2,1,0:T(8,128)(2,1)} %all-gather.3.cloned.1.call-done, f32[4,256]{1,0:T(4,128)S(1)} %bitcast.91), kind=kOutput, calls=%fused_computation.14 | convolution fusion | flops 1074003968 | bytes 6295552 | tf_op jit(solution)/shard_map/secd,edf->secf/dot_general | solution.py:55
  109.2 20.8 %all-to-all-done.1 = bf16[4,512,256]{2,1,0:T(8,128)(2,1)S(1)} async-done(((bf16[4,512,256]{2,1,0:T(8,128)(2,1)}), bf16[4,512,256]{2,1,0:T(8,128)(2,1)S(1)}, u32[]{:S(2)}, u32[]{:S(2)}) %all-to-all-start.1) | async-done | bytes 1048608 | tf_op jit(solution)/shard_map/all_to_all | solution.py:12
  130.1 4.5 %fusion.6 = bf16[4,256,256]{1,2,0:T(8,128)(2,1)} fusion(bf16[2048,256,1]{1,0,2:T(8,128)(2,1)S(1)} %bitcast.80, bf16[4,256,2048]{2,1,0:T(8,128)(2,1)} %all-gather.3.cloned.1.call-done, f32[4,1,256,256]{2,3,0,1:T(8,128)S(1)} %fusion.3, f32[4,256]{1,0:T(4,128)S(1)} %bitcast.92, f32[4,256]{1,0:T(4,128)S(1)} %bitcast.90), kind=kOutput, calls=%fused_computation.17 | convolution fusion | flops 1075838976 | bytes 6823936 | tf_op jit(solution)/shard_map/secd,edf->secf/dot_general | solution.py:56
  134.6 3.5 %all-to-all-start.5 = ((bf16[4,256,256]{1,2,0:T(8,128)(2,1)}), bf16[4,256,256]{1,2,0:T(8,128)(2,1)S(1)}, u32[]{:S(2)}, u32[]{:S(2)}) async-start(bf16[4,256,256]{1,2,0:T(8,128)(2,1)} %fusion.6), calls=%async_computation.5 | async-start | bytes 1048576 | tf_op jit(solution)/shard_map/all_to_all | solution.py:65
  138.1 14.0 %all-to-all-done.5 = bf16[4,256,256]{1,2,0:T(8,128)(2,1)S(1)} async-done(((bf16[4,256,256]{1,2,0:T(8,128)(2,1)}), bf16[4,256,256]{1,2,0:T(8,128)(2,1)S(1)}, u32[]{:S(2)}, u32[]{:S(2)}) %all-to-all-start.5) | async-done | bytes 524320 | tf_op jit(solution)/shard_map/all_to_all | solution.py:65
  152.1 0.2 copy.33
  152.3 2.0 %gather_fusion.1 = bf16[512,256]{1,0:T(8,128)(2,1)S(1)} fusion(bf16[1024,256]{1,0:T(8,128)(2,1)S(1)} %bitcast.77, s32[1024]{0:T(1024)S(1)} %pad_clamp_fusion), kind=kCustom, calls=%fused_computation.2 | custom fusion | bytes 526336 | tf_op jit(solution)/shard_map/gather | solution.py:66
  154.2 0.8 reshape.181
  155.0 1.0 copy.46
  156.0 1.0 copy.47
  (18 shorter events, 0.2 us)
Async XLA Ops:
  7.2 98.6 %all-gather.3.cloned.1.call-start = ((), (), s32[]{:S(2)}) async-start(), calls=%async_computation.6 | async-start | bytes 5242880 | tf_op jit(solution)/shard_map/all_gather | solution.py:54
  12.2 37.1 %copy-start.1 = (f32[256,2]{0,1:T(2,128)S(1)}, f32[256,2]{0,1:T(2,128)}, u32[]{:S(2)}) copy-start(f32[256,2]{0,1:T(2,128)} %param.11) | copy-start | bytes 6148
  12.2 44.9 %copy-start = (bf16[256,2048]{1,0:T(8,128)(2,1)S(1)}, bf16[256,2048]{1,0:T(8,128)(2,1)}, u32[]{:S(2)}) copy-start(bf16[256,2048]{1,0:T(8,128)(2,1)} %param.6) | copy-start | bytes 3145732
  49.3 20.5 %copy-start.2 = (f32[512]{0:T(512)S(1)}, f32[512]{0:T(512)}, u32[]{:S(2)}) copy-start(f32[512]{0:T(512)} %param.7) | copy-start | bytes 6148
  53.9 10.8 %all-to-all-start.2 = ((bf16[4,2,128]{2,1,0:T(2,128)(2,1)}), bf16[4,2,128]{2,1,0:T(2,128)(2,1)S(1)}, u32[]{:S(2)}, u32[]{:S(2)}) async-start(bf16[4,2,128]{2,1,0:T(2,128)(2,1)} %reshape.249), calls=%async_computation.2 | async-start | bytes 4096 | tf_op jit(solution)/shard_map/all_to_all | solution.py:48
  64.7 10.5 %all-to-all-start.4 = ((bf16[4,2,128]{2,1,0:T(2,128)(2,1)}), bf16[4,2,128]{2,1,0:T(2,128)(2,1)S(1)}, u32[]{:S(2)}, u32[]{:S(2)}) async-start(bf16[4,2,128]{2,1,0:T(2,128)(2,1)} %reshape.247), calls=%async_computation.4 | async-start | bytes 4096 | tf_op jit(solution)/shard_map/all_to_all | solution.py:45
  101.9 28.1 %all-to-all-start.1 = ((bf16[4,512,256]{2,1,0:T(8,128)(2,1)}), bf16[4,512,256]{2,1,0:T(8,128)(2,1)S(1)}, u32[]{:S(2)}, u32[]{:S(2)}) async-start(bf16[4,512,256]{2,1,0:T(8,128)(2,1)} %get-tuple-element.3), calls=%async_computation.1 | async-start | bytes 2097152 | tf_op jit(solution)/shard_map/all_to_all | solution.py:12
  134.6 17.5 %all-to-all-start.5 = ((bf16[4,256,256]{1,2,0:T(8,128)(2,1)}), bf16[4,256,256]{1,2,0:T(8,128)(2,1)S(1)}, u32[]{:S(2)}, u32[]{:S(2)}) async-start(bf16[4,256,256]{1,2,0:T(8,128)(2,1)} %fusion.6), calls=%async_computation.5 | async-start | bytes 1048576 | tf_op jit(solution)/shard_map/all_to_all | solution.py:65
Sparse Core Ops, SparseCore 0:
  49.4 33.5 all-gather.2
where the time goes:
time: 164 us
  blocking collectives  58.7 us (36%)
  waiting for transfers between devices  36.8 us (22%)
  local copies, waits for them, and re-layouts  23.1 us (14%)
  starting transfers between devices  15.5 us (9%)
  between operations  14.3 us (9%)
  matrix products  7.99 us (5%)
  other arithmetic  7.42 us (5%)
    all_to_all x1, blocking collectives, on_device(): lax.all_to_all(row_buf, 'fs', split_axis=0, concat_axis=0, tiled=True)  32 us
    all_to_all x1, blocking collectives, on_device(): lax.all_to_all(folded_gate, 'fs', split_axis=0, concat_axis=1, tiled=True)  26.7 us
    all_to_all x1, waiting for transfers between devices, on_device(): lax.all_to_all(folded_up, 'fs', split_axis=0, concat_axis=1, tiled=True)  20.8 us
    all_to_all x1, waiting for transfers between devices, on_device(): lax.all_to_all(hidden_rows, 'fs', split_axis=0, concat_axis=0, tiled=True)  14 us
    all_to_all x1, starting transfers between devices, on_device(): lax.all_to_all(scale_buf.astype(jnp.bfloat16), 'fs', split_axis=0, concat...  5.05 us
    scatter x1, local copies, waits for them, and re-layouts, on_device(): jnp.zeros((total, narrow), jnp.bfloat16).at[target].set(own_cols[owner])  5.05 us
    dot_general x1, matrix products, on_device(): jnp.einsum('secd,edf->secf', piece, new_up, preferred_element_type=jnp.fl...  4.48 us
    unnamed x15, local copies, waits for them, and re-layouts  3.97 us
  transfers between devices with their start and end apart: 5, of which 3 were waited for; matrix products, arithmetic and copies ran while one was open for 12% of the time, Pallas kernels for 0%

commit v1 on v0

--- a/solution.py
+++ b/solution.py
@@ -62,7 +62,19 @@
     up = up * factor
     hidden_rows = (weight * jax.nn.silu(gate) * up).astype(jnp.bfloat16)
     hidden_rows = hidden_rows.reshape(sources * local, capacity, hidden_rows.shape[3])
-    back = lax.all_to_all(hidden_rows, "fs", split_axis=0, concat_axis=0, tiled=True)
+    ways, here = (lax.axis_size("fs"), lax.axis_index("fs"))
+    width_2 = hidden_rows.shape[0] // ways
+    shape = list(hidden_rows.shape)
+    shape[0] = width_2
+    height = shape[0]
+    shape[0] = height * ways
+    full = jnp.zeros(shape, hidden_rows.dtype)
+    for mask in range(ways):
+        part = lax.dynamic_slice_in_dim(hidden_rows, (here ^ mask) * width_2, width_2, axis=0)
+        if mask:
+            part = lax.ppermute(part, "fs", [(d, d ^ mask) for d in range(ways)])
+        full = lax.dynamic_update_slice_in_dim(full, part, (here ^ mask) * height, axis=0)
+    back = full
     picked = back.reshape(total, back.shape[2])[target].reshape(tok_rows, top, back.shape[2])
     return (new_gate, new_up, picked)
 

time: 164 us -> 159 us (0.970)
  waiting for transfers between devices: 36.8 us -> 31.4 us
    all_to_all x1 -> x0, waiting for transfers between devices: 14 us -> none  [on_device(): lax.all_to_all(hidden_rows, 'fs', split_axis=0, concat_axis=0, tiled=True)]
    ppermute x0 -> x3, waiting for transfers between devices: none -> 8.08 us  [on_device(): part = lax.ppermute(part, 'fs', [(d, d ^ mask) for d in range(ways)])]
    ppermute x0 -> x3, starting transfers between devices: none -> 4.38 us  [on_device(): part = lax.ppermute(part, 'fs', [(d, d ^ mask) for d in range(ways)])]
    all_to_all x1 -> x0, starting transfers between devices: 3.47 us -> none  [on_device(): lax.all_to_all(hidden_rows, 'fs', split_axis=0, concat_axis=0, tiled=True)]
    all_to_all x1, waiting for transfers between devices: 0.01 us -> 1.95 us  [on_device(): lax.all_to_all(share_buf.astype(jnp.bfloat16), 'fs', split_axis=0, concat...]
    all_to_all x1, starting transfers between devices: 5.05 us -> 3.22 us  [on_device(): lax.all_to_all(scale_buf.astype(jnp.bfloat16), 'fs', split_axis=0, concat...]
  transfers between devices with their start and end apart: 5 -> 7, of which waited for: 3 -> 5; matrix products, arithmetic and copies ran while one was open for 12% -> 13% of each run, Pallas kernels for 0% -> 0%
where the time goes in v1:
time: 159 us
  blocking collectives  58.7 us (37%)
  waiting for transfers between devices  31.4 us (20%)
  local copies, waits for them, and re-layouts  23.7 us (15%)
  starting transfers between devices  15 us (9%)
  between operations  14.3 us (9%)
  matrix products  8.21 us (5%)
  other arithmetic  7.41 us (5%)
    all_to_all x1, blocking collectives, on_device(): lax.all_to_all(row_buf, 'fs', split_axis=0, concat_axis=0, tiled=True)  32 us
    all_to_all x1, blocking collectives, on_device(): lax.all_to_all(folded_gate, 'fs', split_axis=0, concat_axis=1, tiled=True)  26.7 us
    all_to_all x1, waiting for transfers between devices, on_device(): lax.all_to_all(folded_up, 'fs', split_axis=0, concat_axis=1, tiled=True)  19.9 us
    ppermute x3, waiting for transfers between devices, on_device(): part = lax.ppermute(part, 'fs', [(d, d ^ mask) for d in range(ways)])  8.08 us
    scatter x1, local copies, waits for them, and re-layouts, on_device(): jnp.zeros((total, narrow), jnp.bfloat16).at[target].set(own_cols[owner])  5.05 us
    dot_general x1, matrix products, on_device(): jnp.einsum('secd,edf->secf', piece, new_gate, preferred_element_type=jnp....  4.41 us
    ppermute x3, starting transfers between devices, on_device(): part = lax.ppermute(part, 'fs', [(d, d ^ mask) for d in range(ways)])  4.38 us
    unnamed x15, local copies, waits for them, and re-layouts  3.97 us
  transfers between devices with their start and end apart: 7, of which 5 were waited for; matrix products, arithmetic and copies ran while one was open for 13% of the time, Pallas kernels for 0%

profile of v1, /device:TPU:0, one launch (start us, length us, event | category | flops | bytes accessed | tf_op | source)
XLA Modules:
  0.0 158.7 jit_solution(7901068330641729198)
XLA Ops:
  7.2 0.0 all-gather.3.cloned.1.call-start
  7.2 0.8 copy.18
  8.0 0.1 eq.29
  8.2 0.1 eq.25
  8.3 0.7 broadcast_multiply_fusion
  9.0 1.2 reduce-window.6
  10.2 0.2 slice_reduce_fusion
  10.4 0.2 reduce-window.9
  10.6 0.1 add_bitcast_fusion
  10.7 0.1 copy.17
  10.8 0.1 mul.75
  11.0 0.1 reshape.176
  11.2 1.0 constant_dynamic-slice_fusion
  12.2 0.0 copy-start
  12.2 5.0 %scatter_custom_fusion.1 = bf16[1024,512]{1,0:T(8,128)(2,1)S(1)} fusion(s32[512]{0:T(512)S(1)} %bitcast.80, bf16[256,512]{1,0:T(8,128)(2,1)S(1)} %constant_dynamic-slice_fusion, s32[1024]{0:T(1024)S(1)} %pad_clamp_fusion.1, bf16[]{:T(256)} %constant.16.clone.1), kind=kCustom, calls=%fused_computation.17 | custom fusion | bytes 1048578 | tf_op jit(solution)/shard_map/scatter | solution.py:41
  17.2 32.0 %all_to_all.41 = bf16[4,256,512]{2,1,0:T(8,128)(2,1)} all-to-all(bf16[4,256,512]{2,1,0:T(8,128)(2,1)S(1)} %bitcast.79), channel_id=1, replica_groups=mesh['grp'=2,'fs'=4,'tp'=4] {'fs'}, dimensions={0} | all-to-all | bytes 2097152 | tf_op jit(solution)/shard_map/all_to_all | solution.py:44
  49.2 0.0 copy-start.1
  49.2 0.0 copy-start.2
  49.2 0.0 all-gather.3.cloned.1.call-update
  49.3 0.0 copy-done
  49.3 0.3 multiply_reduce_fusion
  49.6 3.5 %gather_fusion = f32[512]{0:T(512)S(1)} fusion(f32[256]{0:T(256)S(1)} %add_rsqrt_fusion, s32[1024]{0:T(1024)S(1)} %pad_clamp_fusion.1), kind=kCustom, calls=%fused_computation.1 | custom fusion | bytes 6144 | tf_op jit(solution)/shard_map/gather | solution.py:31
  53.1 2.4 %scatter_custom_fusion.2 = f32[1024]{0:T(1024)S(1)} fusion(s32[512]{0:T(512)S(1)} %bitcast.81, f32[512]{0:T(512)S(1)} %gather_fusion, f32[]{:T(128)} %constant.17.clone.1), kind=kCustom, calls=%fused_computation.43 | custom fusion | bytes 4100 | tf_op jit(solution)/shard_map/scatter | solution.py:31
  55.6 0.5 broadcast.103
  56.1 0.7 reduce.2
  56.8 0.6 reshape.248
  57.3 3.2 %all-to-all-start.4 = ((bf16[4,2,128]{2,1,0:T(2,128)(2,1)}), bf16[4,2,128]{2,1,0:T(2,128)(2,1)S(1)}, u32[]{:S(2)}, u32[]{:S(2)}) async-start(bf16[4,2,128]{2,1,0:T(2,128)(2,1)} %reshape.248), calls=%async_computation.4 | async-start | bytes 4096 | tf_op jit(solution)/shard_map/all_to_all | solution.py:45
  60.6 0.0 copy-done.1
  60.6 0.1 copy.20
  60.8 0.1 reshape.213
  60.9 2.4 %scatter_custom_fusion = f32[1024]{0:T(1024)S(1)} fusion(s32[512]{0:T(512)S(1)} %bitcast.82, f32[512]{0:T(512)S(1)} %reshape.213, f32[]{:T(128)} %constant.17.clone.1), kind=kCustom, calls=%fused_computation.45 | custom fusion | bytes 4100 | tf_op jit(solution)/shard_map/scatter | solution.py:36
  63.4 0.7 reduce.3
  64.1 0.6 reshape.250
  64.6 1.4 all-to-all-done.4
  66.0 3.7 %all-to-all-start.2 = ((bf16[4,2,128]{2,1,0:T(2,128)(2,1)}), bf16[4,2,128]{2,1,0:T(2,128)(2,1)S(1)}, u32[]{:S(2)}, u32[]{:S(2)}) async-start(bf16[4,2,128]{2,1,0:T(2,128)(2,1)} %reshape.250), calls=%async_computation.2 | async-start | bytes 4096 | tf_op jit(solution)/shard_map/all_to_all | solution.py:48
  69.7 0.0 copy-done.2
  69.7 3.5 %multiply_convert_fusion = (bf16[4,512,256]{2,1,0:T(8,128)(2,1)}, bf16[4,512,256]{2,1,0:T(8,128)(2,1)S(1)}) fusion(f32[4,512,256]{2,1,0:T(8,128)} %param.9, f32[512]{0:T(512)S(1)} %copy-done.2, f32[4,512,256]{2,1,0:T(8,128)} %param.8), kind=kLoop, calls=%fused_computation.7 | loop fusion | flops 2097152 | bytes 6293504 | tf_op jit(solution)/shard_map/convert_element_type | solution.py:9
  73.2 2.0 %all-to-all-done.2 = bf16[4,2,128]{2,1,0:T(2,128)(2,1)S(1)} async-done(((bf16[4,2,128]{2,1,0:T(2,128)(2,1)}), bf16[4,2,128]{2,1,0:T(2,128)(2,1)S(1)}, u32[]{:S(2)}, u32[]{:S(2)}) %all-to-all-start.2) | async-done | bytes 2080 | tf_op jit(solution)/shard_map/all_to_all | solution.py:48
  75.2 26.7 %all_to_all.42 = bf16[4,512,256]{2,1,0:T(8,128)(2,1)S(1)} all-to-all(bf16[4,512,256]{2,1,0:T(8,128)(2,1)S(1)} %get-tuple-element.7), channel_id=1, replica_groups=mesh['grp'=2,'fs'=4,'tp'=4] {'fs'}, dimensions={0} | all-to-all | bytes 2097152 | tf_op jit(solution)/shard_map/all_to_all | solution.py:11
  101.9 3.7 %all-to-all-start.1 = ((bf16[4,512,256]{2,1,0:T(8,128)(2,1)}), bf16[4,512,256]{2,1,0:T(8,128)(2,1)S(1)}, u32[]{:S(2)}, u32[]{:S(2)}) async-start(bf16[4,512,256]{2,1,0:T(8,128)(2,1)} %get-tuple-element.6), calls=%async_computation.1 | async-start | bytes 2097152 | tf_op jit(solution)/shard_map/all_to_all | solution.py:12
  105.7 0.0 all-gather.3.cloned.1.call-done
  105.7 4.4 %fusion.3 = f32[4,1,256,256]{3,2,0,1:T(8,128)} fusion(bf16[2048,256,1]{1,0,2:T(8,128)(2,1)S(1)} %bitcast.75, bf16[4,256,2048]{2,1,0:T(8,128)(2,1)} %all-gather.3.cloned.1.call-done, f32[4,256]{1,0:T(4,128)S(1)} %bitcast.87), kind=kOutput, calls=%fused_computation.14 | convolution fusion | flops 1074003968 | bytes 6295552 | tf_op jit(solution)/shard_map/secd,edf->secf/dot_general | solution.py:55
  110.1 19.9 %all-to-all-done.1 = bf16[4,512,256]{2,1,0:T(8,128)(2,1)S(1)} async-done(((bf16[4,512,256]{2,1,0:T(8,128)(2,1)}), bf16[4,512,256]{2,1,0:T(8,128)(2,1)S(1)}, u32[]{:S(2)}, u32[]{:S(2)}) %all-to-all-start.1) | async-done | bytes 1048608 | tf_op jit(solution)/shard_map/all_to_all | solution.py:12
  130.1 3.8 %fusion.5 = bf16[4,1,256,256]{3,2,0,1:T(8,128)(2,1)S(1)} fusion(bf16[2048,256,1]{1,0,2:T(8,128)(2,1)S(1)} %bitcast.77, bf16[4,256,2048]{2,1,0:T(8,128)(2,1)} %all-gather.3.cloned.1.call-done, f32[4,1,256,256]{3,2,0,1:T(8,128)} %fusion.3, f32[4,256]{1,0:T(4,128)S(1)} %bitcast.88, f32[4,256]{1,0:T(4,128)S(1)} %bitcast.89), kind=kOutput, calls=%fused_computation.16 | convolution fusion | flops 1075838976 | bytes 6823936 | tf_op jit(solution)/shard_map/secd,edf->secf/dot_general | solution.py:56
  133.9 0.7 dynamic-slice_bitcast_fusion
  134.6 0.0 collective-permute-start
  134.6 2.0 %collective-permute-start.1 = (bf16[1,256,256]{2,1,0:T(8,128)(2,1)S(1)}, bf16[1,256,256]{2,1,0:T(8,128)(2,1)S(1)}, u32[]{:S(2)}, u32[]{:S(2)}) collective-permute-start(bf16[1,256,256]{2,1,0:T(8,128)(2,1)S(1)} %get-tuple-element.4), channel_id=1, source_target_pairs={{0,8},{4,12},{8,0},{12,4},{1,9},{5,13},{9,1},{13,5},{2,10},{6,14},... | collective-permute-start | bytes 393224 | tf_op jit(solution)/shard_map/ppermute | solution.py:75
  136.6 2.4 %collective-permute-start.2 = (bf16[1,256,256]{2,1,0:T(8,128)(2,1)S(1)}, bf16[1,256,256]{2,1,0:T(8,128)(2,1)S(1)}, u32[]{:S(2)}, u32[]{:S(2)}) collective-permute-start(bf16[1,256,256]{2,1,0:T(8,128)(2,1)S(1)} %get-tuple-element.3), channel_id=1, source_target_pairs={{0,12},{4,8},{8,4},{12,0},{1,13},{5,9},{9,5},{13,1},{2,14},{6,10},... | collective-permute-start | bytes 393224 | tf_op jit(solution)/shard_map/ppermute | solution.py:75
  139.0 2.1 %collective-permute-done = bf16[1,256,256]{2,1,0:T(8,128)(2,1)S(1)} collective-permute-done((bf16[1,256,256]{2,1,0:T(8,128)(2,1)}, bf16[1,256,256]{2,1,0:T(8,128)(2,1)S(1)}, u32[]{:S(2)}, u32[]{:S(2)}) %collective-permute-start) | collective-permute-done | bytes 131104 | tf_op jit(solution)/shard_map/ppermute | solution.py:75
  141.2 5.9 %collective-permute-done.1 = bf16[1,256,256]{2,1,0:T(8,128)(2,1)S(1)} collective-permute-done((bf16[1,256,256]{2,1,0:T(8,128)(2,1)S(1)}, bf16[1,256,256]{2,1,0:T(8,128)(2,1)S(1)}, u32[]{:S(2)}, u32[]{:S(2)}) %collective-permute-start.1) | collective-permute-done | bytes 131104 | tf_op jit(solution)/shard_map/ppermute | solution.py:75
  147.1 0.0 collective-permute-done.2
  147.2 2.0 %gather_fusion.1 = bf16[512,256]{1,0:T(8,128)(2,1)S(1)} fusion(bf16[1024,256]{1,0:T(8,128)(2,1)S(1)} %bitcast.74, s32[1024]{0:T(1024)S(1)} %pad_clamp_fusion), kind=kCustom, calls=%fused_computation.2 | custom fusion | bytes 526336 | tf_op jit(solution)/shard_map/gather | solution.py:78
  149.1 0.8 reshape.182
  149.9 1.0 copy.37
  150.9 1.0 copy.38
  (22 shorter events, 0.3 us)
Async XLA Ops:
  7.2 98.5 %all-gather.3.cloned.1.call-start = ((), (), s32[]{:S(2)}) async-start(), calls=%async_computation.5 | async-start | bytes 5242880 | tf_op jit(solution)/shard_map/all_gather | solution.py:54
  12.2 37.1 %copy-start = (bf16[256,2048]{1,0:T(8,128)(2,1)S(1)}, bf16[256,2048]{1,0:T(8,128)(2,1)}, u32[]{:S(2)}) copy-start(bf16[256,2048]{1,0:T(8,128)(2,1)} %param.6) | copy-start | bytes 3145732
  49.2 11.4 %copy-start.1 = (f32[256,2]{0,1:T(2,128)S(1)}, f32[256,2]{0,1:T(2,128)}, u32[]{:S(2)}) copy-start(f32[256,2]{0,1:T(2,128)} %param.11) | copy-start | bytes 6148
  49.2 20.5 %copy-start.2 = (f32[512]{0:T(512)S(1)}, f32[512]{0:T(512)}, u32[]{:S(2)}) copy-start(f32[512]{0:T(512)} %param.7) | copy-start | bytes 6148
  57.3 8.7 %all-to-all-start.4 = ((bf16[4,2,128]{2,1,0:T(2,128)(2,1)}), bf16[4,2,128]{2,1,0:T(2,128)(2,1)S(1)}, u32[]{:S(2)}, u32[]{:S(2)}) async-start(bf16[4,2,128]{2,1,0:T(2,128)(2,1)} %reshape.248), calls=%async_computation.4 | async-start | bytes 4096 | tf_op jit(solution)/shard_map/all_to_all | solution.py:45
  66.0 9.2 %all-to-all-start.2 = ((bf16[4,2,128]{2,1,0:T(2,128)(2,1)}), bf16[4,2,128]{2,1,0:T(2,128)(2,1)S(1)}, u32[]{:S(2)}, u32[]{:S(2)}) async-start(bf16[4,2,128]{2,1,0:T(2,128)(2,1)} %reshape.250), calls=%async_computation.2 | async-start | bytes 4096 | tf_op jit(solution)/shard_map/all_to_all | solution.py:48
  101.9 28.2 %all-to-all-start.1 = ((bf16[4,512,256]{2,1,0:T(8,128)(2,1)}), bf16[4,512,256]{2,1,0:T(8,128)(2,1)S(1)}, u32[]{:S(2)}, u32[]{:S(2)}) async-start(bf16[4,512,256]{2,1,0:T(8,128)(2,1)} %get-tuple-element.6), calls=%async_computation.1 | async-start | bytes 2097152 | tf_op jit(solution)/shard_map/all_to_all | solution.py:12
  134.6 6.6 %collective-permute-start = (bf16[1,256,256]{2,1,0:T(8,128)(2,1)}, bf16[1,256,256]{2,1,0:T(8,128)(2,1)S(1)}, u32[]{:S(2)}, u32[]{:S(2)}) collective-permute-start(bf16[1,256,256]{2,1,0:T(8,128)(2,1)} %get-tuple-element.5), channel_id=1, source_target_pairs={{0,4},{4,0},{8,12},{12,8},{1,5},{5,1},{9,13},{13,9},{2,6},{6,2},{1... | collective-permute-start | bytes 393224 | tf_op jit(solution)/shard_map/ppermute | solution.py:75
  134.6 12.5 %collective-permute-start.1 = (bf16[1,256,256]{2,1,0:T(8,128)(2,1)S(1)}, bf16[1,256,256]{2,1,0:T(8,128)(2,1)S(1)}, u32[]{:S(2)}, u32[]{:S(2)}) collective-permute-start(bf16[1,256,256]{2,1,0:T(8,128)(2,1)S(1)} %get-tuple-element.4), channel_id=1, source_target_pairs={{0,8},{4,12},{8,0},{12,4},{1,9},{5,13},{9,1},{13,5},{2,10},{6,14},... | collective-permute-start | bytes 393224 | tf_op jit(solution)/shard_map/ppermute | solution.py:75
  136.6 10.5 %collective-permute-start.2 = (bf16[1,256,256]{2,1,0:T(8,128)(2,1)S(1)}, bf16[1,256,256]{2,1,0:T(8,128)(2,1)S(1)}, u32[]{:S(2)}, u32[]{:S(2)}) collective-permute-start(bf16[1,256,256]{2,1,0:T(8,128)(2,1)S(1)} %get-tuple-element.3), channel_id=1, source_target_pairs={{0,12},{4,8},{8,4},{12,0},{1,13},{5,9},{9,5},{13,1},{2,14},{6,10},... | collective-permute-start | bytes 393224 | tf_op jit(solution)/shard_map/ppermute | solution.py:75
Sparse Core Ops, SparseCore 0:
  49.4 33.5 all-gather.2
